TPU v7x, 32 devices: a whole 2x2x4 slice. The times are simulated.
32 devices in a mesh: sp: 8 (over z, y), tp: 4 (over x, core).
Axes of the slice: x: 2, y: 2, z: 4, core: 2. Of those that a mesh axis runs over, the one named last changes fastest.
Arguments:
- query_first: bfloat16 [6144, 8, 128], P('sp', 'tp'), may hold values from -5.375 to 5.375
- key_first: bfloat16 [6144, 8, 128], P('sp', 'tp'), may hold values from -5.375 to 5.375
- value_first: bfloat16 [6144, 8, 128], P('sp', 'tp'), may hold values from -6 to 6
- query_second: bfloat16 [6144, 8, 256], P('sp', 'tp'), may hold values from -5.375 to 5.375
- key_second: bfloat16 [6144, 8, 256], P('sp', 'tp'), may hold values from -5.375 to 5.375
- value_second: bfloat16 [6144, 8, 128], P('sp', 'tp'), may hold values from -6 to 6
- mix_lambda: float32 [2, 8], P(None, 'tp'), may hold values from 0.3 to 0.8
- head_gain: float32 [2, 8, 128], P(None, 'tp'), may hold values from 0.1 to 1.9
- out_weight: bfloat16 [2, 8, 128, 2048], P(None, 'tp'), may hold values from -0.125 to 0.125
- residual: bfloat16 [6144, 2048], P(('sp', 'tp')), may hold values from -6 to 6
- norm_gain: float32 [2, 2048], replicated, may hold values from 0.1 to 1.9
- up_weight: bfloat16 [2048, 8192], P('sp', 'tp'), may hold values from -0.125 to 0.125
- down_weight: bfloat16 [8192, 2048], P('tp', 'sp'), may hold values from -0.0625 to 0.0625
Outputs:
- mixed: bfloat16 [6144, 2048], P(('sp', 'tp'))
All inputs are finite; a program needn't handle non-finite values.
Results may differ from a plain program's by a relative error of at most 0.02.
Values may be sent and summed in bfloat16 or wider, within the bound.
A program may use at most 128 MiB of HBM per device.

v0:
```python
import math
import jax
import jax.numpy as jnp
from jax import lax
from jax.sharding import PartitionSpec as P

EPSILON = 1e-05
LOWEST = -1e30


def layer_norm(activations, scales):
    average = jnp.mean(activations, axis=-1, keepdims=True)
    centred = activations - average
    spread = jnp.mean(centred * centred, axis=-1, keepdims=True)
    return centred * lax.rsqrt(spread + EPSILON) * scales


def fold_group(carried, queries, key_rows, values, score_scale):
    maxima, totals, numerator = carried
    scores = (
        jnp.einsum("qhck,phck->hcqp", queries, key_rows, preferred_element_type=jnp.float32)
        * score_scale
    )
    newest = jnp.maximum(maxima, jnp.max(scores, axis=-1))
    weights = jnp.exp(scores - newest[..., None])
    factor = jnp.exp(maxima - newest)
    totals = totals * factor + jnp.sum(weights, axis=-1)
    numerator = numerator * factor[..., None] + jnp.einsum(
        "hcqp,phv->hcqv", weights.astype(jnp.bfloat16), values, preferred_element_type=jnp.float32
    )
    return (newest, totals, numerator)


def finish_group(carried, lambdas, gains):
    maxima, totals, numerator = carried
    attended = (
        numerator[:, 0] / totals[:, 0, :, None]
        - lambdas[:, None, None] * numerator[:, 1] / totals[:, 1, :, None]
    )
    mean_square = jnp.mean(attended * attended, axis=-1, keepdims=True)
    return (attended * lax.rsqrt(mean_square + EPSILON) * gains[:, None, :]).astype(jnp.bfloat16)


def squared_relu(expanded):
    return jnp.square(jnp.maximum(expanded, 0.0)).astype(jnp.bfloat16)


def local(
    query_first,
    key_first,
    value_first,
    query_second,
    key_second,
    value_second,
    mix_lambda,
    head_gain,
    out_weight,
    residual,
    norm_gain,
    up_weight,
    down_weight,
):
    up_whole, down_whole = (
        lax.all_gather(up_weight, "sp", axis=0, tiled=True),
        lax.all_gather(down_weight, "sp", axis=1, tiled=True),
    )
    tok_dev, local_heads, width_first = query_first.shape
    size_first = width_first // 2
    size_second = query_second.shape[2] // 2
    value_size = value_first.shape[2]
    scale_first = 1.0 / math.sqrt(size_first)
    scale_second = 1.0 / math.sqrt(size_second)
    queries_first = query_first.reshape(tok_dev, local_heads, 2, size_first)
    queries_second = query_second.reshape(tok_dev, local_heads, 2, size_second)

    def initial():
        return (
            jnp.full((local_heads, 2, tok_dev), LOWEST, jnp.float32),
            jnp.zeros((local_heads, 2, tok_dev), jnp.float32),
            jnp.zeros((local_heads, 2, tok_dev, value_size), jnp.float32),
        )

    carried = (initial(), initial())
    pieces = (
        lax.all_gather(key_first, "sp", axis=0, tiled=True),
        lax.all_gather(key_second, "sp", axis=0, tiled=True),
        lax.all_gather(value_first, "sp", axis=0, tiled=True),
        lax.all_gather(value_second, "sp", axis=0, tiled=True),
    )
    length = pieces[0].shape[0]
    block_count = length // tok_dev
    segments = tuple(
        (member.reshape((block_count, tok_dev) + member.shape[1:]) for member in pieces)
    )

    def absorb_block(running, segment):
        keys_one, keys_two, values_one, values_two = segment
        first_state = fold_group(
            running[0],
            queries_first,
            keys_one.reshape(tok_dev, local_heads, 2, size_first),
            values_one,
            scale_first,
        )
        second_state = fold_group(
            running[1],
            queries_second,
            keys_two.reshape(tok_dev, local_heads, 2, size_second),
            values_two,
            scale_second,
        )
        return ((first_state, second_state), None)

    carried, unused = lax.scan(absorb_block, carried, segments)
    state_first, state_second = carried
    heads_first = finish_group(state_first, mix_lambda[0], head_gain[0])
    heads_second = finish_group(state_second, mix_lambda[1], head_gain[1])
    stacked = jnp.stack([heads_first, heads_second])
    selected = stacked
    projected = lax.psum_scatter(
        jnp.einsum(
            "ghqv,ghvd->qd", selected, out_weight, preferred_element_type=jnp.float32
        ).astype(jnp.bfloat16),
        "tp",
        scatter_dimension=0,
        tiled=True,
    ).astype(jnp.float32) + residual.astype(jnp.float32)
    normed = layer_norm(projected, norm_gain[0])
    mixer_in = lax.all_gather(normed.astype(jnp.bfloat16), "tp", axis=0, tiled=True)
    hidden = squared_relu(jnp.dot(mixer_in, up_whole, preferred_element_type=jnp.float32))
    selected = hidden
    mixed_sum = lax.psum_scatter(
        jnp.dot(selected, down_whole, preferred_element_type=jnp.float32).astype(jnp.bfloat16),
        "tp",
        scatter_dimension=0,
        tiled=True,
    ).astype(jnp.float32)
    return layer_norm(normed + mixed_sum, norm_gain[1]).astype(jnp.bfloat16)


def solution(mesh):
    return jax.shard_map(
        local,
        mesh=mesh,
        in_specs=(
            P("sp", "tp", None),
            P("sp", "tp", None),
            P("sp", "tp", None),
            P("sp", "tp", None),
            P("sp", "tp", None),
            P("sp", "tp", None),
            P(None, "tp"),
            P(None, "tp", None),
            P(None, "tp", None, None),
            P(("sp", "tp"), None),
            P(),
            P("sp", "tp"),
            P("tp", "sp"),
        ),
        out_specs=P(("sp", "tp"), None),
        check_vma=False,
    )
```

profile of v0, /device:TPU:0, one launch (start us, length us, event | category | flops | bytes accessed | tf_op | source)
XLA Modules:
  0.0 893.3 jit_solution(1156918713239734366)
XLA Ops:
  18.3 54.0 %all-gather.8.cloned.1.call-done = bf16[6144,2,128]{2,0,1:T(8,128)(2,1)} async-done(((bf16[768,2,128]{2,0,1:T(8,128)(2,1)}), bf16[6144,2,128]{2,0,1:T(8,128)(2,1)}) %all-gather.8.cloned.1.call-update) | async-done | bytes 3145744 | tf_op jit(solution)/shard_map/all_gather | solution.py:85
  72.3 60.9 %all-gather.10.cloned.1.call-done = bf16[6144,2,128]{2,0,1:T(8,128)(2,1)} async-done(((bf16[768,2,128]{2,0,1:T(8,128)(2,1)}), bf16[6144,2,128]{2,0,1:T(8,128)(2,1)}) %all-gather.10.cloned.1.call-update) | async-done | bytes 3145744 | tf_op jit(solution)/shard_map/all_gather | solution.py:87
  133.2 60.9 %all-gather.14.cloned.1.call-done = bf16[6144,2,128]{2,0,1:T(8,128)(2,1)} async-done(((bf16[768,2,128]{2,0,1:T(8,128)(2,1)}), bf16[6144,2,128]{2,0,1:T(8,128)(2,1)}) %all-gather.14.cloned.1.call-update) | async-done | bytes 3145744 | tf_op jit(solution)/shard_map/all_gather | solution.py:88
  194.1 99.4 %all-gather.12.cloned.1.call-done = bf16[6144,2,256]{2,0,1:T(8,128)(2,1)} async-done(((bf16[768,2,256]{2,0,1:T(8,128)(2,1)}), bf16[6144,2,256]{2,0,1:T(8,128)(2,1)}) %all-gather.12.cloned.1.call-update) | async-done | bytes 6291472 | tf_op jit(solution)/shard_map/all_gather | solution.py:86
  293.6 214.6 %while.21 = (s32[]{:T(128)}, f32[2,2,768]{2,1,0:T(2,128)S(1)}, f32[2,2,768]{2,1,0:T(2,128)}, f32[2,2,768,128]{3,2,1,0:T(8,128)}, f32[2,2,768]{2,1,0:T(2,128)S(1)...) while((s32[]{:T(128)}, f32[2,2,768]{2,1,0:T(2,128)S(1)}, ...), condition=%wide.region_5.6_spmd.clone, body=%wide.region_0.5_spmd.clone.sunk | while | flops 2154067968 | bytes 149816656 | solution.py:114
  309.2 4.8 fusion.103
  314.0 3.8 fusion.102
  336.1 4.9 fusion.103
  363.1 4.9 fusion.103
  368.1 3.8 fusion.102
  390.2 4.9 fusion.103
  395.1 3.8 fusion.102
  417.2 4.9 fusion.103
  422.1 3.8 fusion.102
  444.2 4.9 fusion.103
  471.2 4.9 fusion.103
  498.3 4.9 fusion.103
  517.9 35.5 %reduce-scatter.3.cloned.1.call-done = bf16[192,2048]{1,0:T(8,128)(2,1)} async-done(((bf16[768,2048]{1,0:T(8,128)(2,1)}), bf16[192,2048]{1,0:T(8,128)(2,1)}) %reduce-scatter.3.cloned.1.call-update) | async-done | bytes 786448 | tf_op jit(solution)/shard_map/reduce_scatter | solution.py:120
  557.4 122.5 %all-gather.18.cloned.1.call-done = bf16[2048,2048]{1,0:T(8,128)(2,1)} async-done(((bf16[256,2048]{1,0:T(8,128)(2,1)}), bf16[2048,2048]{1,0:T(8,128)(2,1)}) %all-gather.18.cloned.1.call-update) | async-done | bytes 8388624 | tf_op jit(solution)/shard_map/all_gather | solution.py:64
  679.9 28.3 %all-gather.16.cloned.1.call-done = bf16[768,2048]{1,0:T(8,128)(2,1)} async-done(((bf16[192,2048]{1,0:T(8,128)(2,1)}), bf16[768,2048]{1,0:T(8,128)(2,1)}) %all-gather.16.cloned.1.call-update) | async-done | bytes 3145744 | tf_op jit(solution)/shard_map/all_gather | solution.py:129
  708.2 11.9 %multiply_convert_fusion = bf16[768,2048]{1,0:T(8,128)(2,1)} fusion(bf16[768,2048]{1,0:T(8,128)(2,1)} %all-gather.16.cloned.1.call-done, bf16[2048,2048]{1,0:T(8,128)(2,1)} %all-gather.18.cloned.1.call-done), kind=kOutput, calls=%fused_computation.41 | convolution fusion | flops 6447169536 | bytes 14680064 | tf_op jit(solution)/shard_map/dot_general | solution.py:130
  720.0 115.2 %all-gather.20.cloned.1.call-done = bf16[2048,2048]{1,0:T(8,128)(2,1)} async-done(((bf16[2048,256]{1,0:T(8,128)(2,1)}), bf16[2048,2048]{1,0:T(8,128)(2,1)}) %all-gather.20.cloned.1.call-update) | async-done | bytes 8388624 | tf_op jit(solution)/shard_map/all_gather | solution.py:65
  835.2 11.8 %convolution_convert_fusion = bf16[768,2048]{1,0:T(8,128)(2,1)} fusion(bf16[768,2048]{1,0:T(8,128)(2,1)} %multiply_convert_fusion, bf16[2048,2048]{1,0:T(8,128)(2,1)} %all-gather.20.cloned.1.call-done), kind=kOutput, calls=%fused_computation.42 | convolution fusion | flops 6444023808 | bytes 14680064 | tf_op jit(solution)/shard_map/dot_general | solution.py:133
  847.1 36.2 %reduce-scatter.5.cloned.1.call-done = bf16[192,2048]{1,0:T(8,128)(2,1)} async-done(((bf16[768,2048]{1,0:T(8,128)(2,1)}), bf16[192,2048]{1,0:T(8,128)(2,1)}) %reduce-scatter.5.cloned.1.call-update) | async-done | bytes 786448 | tf_op jit(solution)/shard_map/reduce_scatter | solution.py:132
  (296 shorter events, 188.2 us)
Async XLA Ops:
  6.5 507.4 %copy-start = (bf16[2,2,128,2048]{3,2,1,0:T(8,128)(2,1)S(1)}, bf16[2,2,128,2048]{3,2,1,0:T(8,128)(2,1)}, u32[]{:S(2)}) copy-start(bf16[2,2,128,2048]{3,2,1,0:T(8,128)(2,1)} %param.23) | copy-start | bytes 6291460
  6.5 65.8 %all-gather.8.cloned.1.call-start = ((), (), s32[]{:S(2)}) async-start(), calls=%async_computation.2 | async-start | bytes 3538944 | tf_op jit(solution)/shard_map/all_gather | solution.py:85
  8.5 124.7 %all-gather.10.cloned.1.call-start = ((), (), s32[]{:S(2)}) async-start(), calls=%async_computation.3 | async-start | bytes 3538944 | tf_op jit(solution)/shard_map/all_gather | solution.py:87
  10.4 183.7 %all-gather.14.cloned.1.call-start = ((), (), s32[]{:S(2)}) async-start(), calls=%async_computation.5 | async-start | bytes 3538944 | tf_op jit(solution)/shard_map/all_gather | solution.py:88
  11.4 282.2 %all-gather.12.cloned.1.call-start = ((), (), s32[]{:S(2)}) async-start(), calls=%async_computation.4 | async-start | bytes 7077888 | tf_op jit(solution)/shard_map/all_gather | solution.py:86
  12.4 541.0 %reduce-scatter.3.cloned.1.call-start = ((), (), s32[]{:S(2)}) async-start(), calls=%async_computation.6 | async-start | bytes 3932160 | tf_op jit(solution)/shard_map/reduce_scatter | solution.py:120
  332.4 8.6 slice-start
  332.4 8.6 slice-start.1
  359.5 8.6 slice-start
  359.5 8.6 slice-start.1
  386.5 8.6 slice-start
  386.5 8.6 slice-start.1
  413.5 8.6 slice-start
  413.5 8.6 slice-start.1
  440.5 8.6 slice-start
  440.5 8.6 slice-start.1
  467.5 8.6 slice-start
  467.6 8.6 slice-start.1
  494.6 8.6 slice-start
  517.2 36.2 %copy-start.6 = (bf16[192,2048]{1,0:T(8,128)(2,1)S(1)}, bf16[192,2048]{1,0:T(8,128)(2,1)}, u32[]{:S(2)}) copy-start(bf16[192,2048]{1,0:T(8,128)(2,1)} %param.24) | copy-start | bytes 2359300
  517.2 162.7 %all-gather.18.cloned.1.call-start = ((), (), s32[]{:S(2)}) async-start(), calls=%async_computation.8 | async-start | bytes 9437184 | tf_op jit(solution)/shard_map/all_gather | solution.py:64
  517.8 190.4 %all-gather.16.cloned.1.call-start = ((), (), s32[]{:S(2)}) async-start(), calls=%async_computation.7 | async-start | bytes 3932160 | tf_op jit(solution)/shard_map/all_gather | solution.py:129
  556.6 278.6 %all-gather.20.cloned.1.call-start = ((), (), s32[]{:S(2)}) async-start(), calls=%async_computation.9 | async-start | bytes 9437184 | tf_op jit(solution)/shard_map/all_gather | solution.py:65
  557.4 325.9 %reduce-scatter.5.cloned.1.call-start = ((), (), s32[]{:S(2)}) async-start(), calls=%async_computation.10 | async-start | bytes 3932160 | tf_op jit(solution)/shard_map/reduce_scatter | solution.py:132
  (47 other events, 171.6 us)
Sparse Core Ops, SparseCore 0:
  9.5 62.7 all-gather.7
  74.5 58.6 all-gather.9
  135.4 58.6 all-gather.13
  196.2 97.3 all-gather.11
  517.3 36.0 reduce-scatter.2
  555.4 124.4 all-gather.17
  681.5 26.6 all-gather.15
  710.2 124.9 all-gather.19
  847.2 36.0 reduce-scatter.4
where the time goes:
time: 895 us; the launch traced here: 893 us
  waiting for transfers between devices  614 us (69%)
  matrix products  136 us (15%)
  local copies, waits for them, and re-layouts  76 us (8%)
  other arithmetic  52 us (6%)
  between operations  13.5 us (2%)
    all_gather x1, waiting for transfers between devices, local(): lax.all_gather(up_weight, 'sp', axis=0, tiled=True)  122 us
    all_gather x1, waiting for transfers between devices, local(): lax.all_gather(down_weight, 'sp', axis=1, tiled=True)  115 us
    all_gather x1, waiting for transfers between devices, local(): lax.all_gather(key_second, 'sp', axis=0, tiled=True)  99.4 us
    dot_general x16, matrix products, fold_group(): jnp.einsum('hcqp,phv->hcqv', weights.astype(jnp.bfloat16), values, prefer...  69.2 us
    all_gather x1, waiting for transfers between devices, local(): lax.all_gather(value_second, 'sp', axis=0, tiled=True)  60.9 us
    all_gather x1, waiting for transfers between devices, local(): lax.all_gather(value_first, 'sp', axis=0, tiled=True)  60.9 us
    all_gather x1, waiting for transfers between devices, local(): lax.all_gather(key_first, 'sp', axis=0, tiled=True)  54 us
    dot_general x16, matrix products, fold_group(): jnp.einsum('qhck,phck->hcqp', queries, key_rows, preferred_element_type=j...  40.3 us
  transfers between devices with their start and end apart: 9, of which 9 were waited for; matrix products, arithmetic and copies ran while one was open for 3% of the time, Pallas kernels for 0%

commit v1 on v0

--- a/solution.py
+++ b/solution.py
@@ -6,6 +6,11 @@
 
 EPSILON = 1e-05
 LOWEST = -1e30
+
+
+def _enter_rings(x_local, row_dim):
+    met_up = jnp.concatenate(lax.all_gather(x_local, axis_name="sp"), axis=row_dim)
+    return met_up
 
 
 def layer_norm(activations, scales):
@@ -62,7 +67,7 @@
 ):
     up_whole, down_whole = (
         lax.all_gather(up_weight, "sp", axis=0, tiled=True),
-        lax.all_gather(down_weight, "sp", axis=1, tiled=True),
+        _enter_rings(down_weight, 1),
     )
     tok_dev, local_heads, width_first = query_first.shape
     size_first = width_first // 2

time: 895 us -> 902 us (level)
  local copies, waits for them, and re-layouts: 76 us -> 87.8 us
    reshape x0 -> x1, local copies, waits for them, and re-layouts: none -> 11.7 us  [_enter_rings(): jnp.concatenate(lax.all_gather(x_local, axis_name='sp'), axis=row_dim)]
    all_gather x1, waiting for transfers between devices: 122 us -> 113 us  [local(): lax.all_gather(up_weight, 'sp', axis=0, tiled=True)]
where the time goes in v1:
time: 902 us; the launch traced here: 899 us
  waiting for transfers between devices  614 us (68%)
  matrix products  131 us (15%)
  local copies, waits for them, and re-layouts  87.8 us (10%)
  other arithmetic  52 us (6%)
  between operations  13.5 us (1%)
    all_gather x1, waiting for transfers between devices, _enter_rings(): lax.all_gather(x_local, axis_name='sp')  123 us
    all_gather x1, waiting for transfers between devices, local(): lax.all_gather(up_weight, 'sp', axis=0, tiled=True)  113 us
    all_gather x1, waiting for transfers between devices, local(): lax.all_gather(key_second, 'sp', axis=0, tiled=True)  99.4 us
    dot_general x16, matrix products, fold_group(): jnp.einsum('hcqp,phv->hcqv', weights.astype(jnp.bfloat16), values, prefer...  69.1 us
    all_gather x1, waiting for transfers between devices, local(): lax.all_gather(value_second, 'sp', axis=0, tiled=True)  60.9 us
    all_gather x1, waiting for transfers between devices, local(): lax.all_gather(value_first, 'sp', axis=0, tiled=True)  60.9 us
    all_gather x1, waiting for transfers between devices, local(): lax.all_gather(key_first, 'sp', axis=0, tiled=True)  54 us
    dot_general x16, matrix products, fold_group(): jnp.einsum('qhck,phck->hcqp', queries, key_rows, preferred_element_type=j...  40.3 us
  transfers between devices with their start and end apart: 9, of which 9 were waited for; matrix products, arithmetic and copies ran while one was open for 3% of the time, Pallas kernels for 0%

profile of v1, /device:TPU:0, one launch (start us, length us, event | category | flops | bytes accessed | tf_op | source)
XLA Modules:
  0.0 899.3 jit_solution(6496615378212958664)
XLA Ops:
  18.3 54.0 %all-gather.9.cloned.1.call-done = bf16[6144,2,128]{2,0,1:T(8,128)(2,1)} async-done(((bf16[768,2,128]{2,0,1:T(8,128)(2,1)}), bf16[6144,2,128]{2,0,1:T(8,128)(2,1)}) %all-gather.9.cloned.1.call-update) | async-done | bytes 3145744 | tf_op jit(solution)/shard_map/all_gather | solution.py:90
  72.3 60.9 %all-gather.11.cloned.1.call-done = bf16[6144,2,128]{2,0,1:T(8,128)(2,1)} async-done(((bf16[768,2,128]{2,0,1:T(8,128)(2,1)}), bf16[6144,2,128]{2,0,1:T(8,128)(2,1)}) %all-gather.11.cloned.1.call-update) | async-done | bytes 3145744 | tf_op jit(solution)/shard_map/all_gather | solution.py:92
  133.2 60.9 %all-gather.15.cloned.1.call-done = bf16[6144,2,128]{2,0,1:T(8,128)(2,1)} async-done(((bf16[768,2,128]{2,0,1:T(8,128)(2,1)}), bf16[6144,2,128]{2,0,1:T(8,128)(2,1)}) %all-gather.15.cloned.1.call-update) | async-done | bytes 3145744 | tf_op jit(solution)/shard_map/all_gather | solution.py:93
  194.1 99.4 %all-gather.13.cloned.1.call-done = bf16[6144,2,256]{2,0,1:T(8,128)(2,1)} async-done(((bf16[768,2,256]{2,0,1:T(8,128)(2,1)}), bf16[6144,2,256]{2,0,1:T(8,128)(2,1)}) %all-gather.13.cloned.1.call-update) | async-done | bytes 6291472 | tf_op jit(solution)/shard_map/all_gather | solution.py:91
  293.6 214.6 %while.21 = (s32[]{:T(128)}, f32[2,2,768]{2,1,0:T(2,128)S(1)}, f32[2,2,768]{2,1,0:T(2,128)}, f32[2,2,768,128]{3,2,1,0:T(8,128)}, f32[2,2,768]{2,1,0:T(2,128)S(1)...) while((s32[]{:T(128)}, f32[2,2,768]{2,1,0:T(2,128)S(1)}, ...), condition=%wide.region_5.6_spmd.clone, body=%wide.region_0.5_spmd.clone.sunk | while | flops 2154067968 | bytes 149816656 | solution.py:119
  309.2 4.7 fusion.103
  336.1 4.9 fusion.103
  363.2 4.9 fusion.103
  390.2 4.9 fusion.103
  395.1 3.8 fusion.102
  417.2 4.9 fusion.103
  422.1 3.8 fusion.102
  444.2 4.9 fusion.103
  471.3 4.9 fusion.103
  476.2 3.8 fusion.102
  498.3 4.9 fusion.103
  518.6 34.8 %reduce-scatter.3.cloned.1.call-done = bf16[192,2048]{1,0:T(8,128)(2,1)} async-done(((bf16[768,2048]{1,0:T(8,128)(2,1)}), bf16[192,2048]{1,0:T(8,128)(2,1)}) %reduce-scatter.3.cloned.1.call-update) | async-done | bytes 786448 | tf_op jit(solution)/shard_map/reduce_scatter | solution.py:125
  556.7 123.2 %all-gather.21.cloned.1.call-done = bf16[16384,256]{1,0:T(8,128)(2,1)} async-done(((bf16[2048,256]{1,0:T(8,128)(2,1)}), bf16[16384,256]{1,0:T(8,128)(2,1)}) %all-gather.21.cloned.1.call-update) | async-done | bytes 8388624 | tf_op jit(solution)/shard_map/all_gather | solution.py:12
  679.9 11.7 %copy.55 = bf16[2048,8,256]{0,2,1:T(8,128)(2,1)} copy(bf16[2048,8,256]{2,0,1:T(8,128)(2,1)} %bitcast.187) | data formatting | bytes 16777216 | tf_op jit(solution)/shard_map/reshape | solution.py:12
  691.6 113.1 %all-gather.19.cloned.1.call-done = bf16[2048,2048]{1,0:T(8,128)(2,1)} async-done(((bf16[256,2048]{1,0:T(8,128)(2,1)}), bf16[2048,2048]{1,0:T(8,128)(2,1)}) %all-gather.19.cloned.1.call-update) | async-done | bytes 8388624 | tf_op jit(solution)/shard_map/all_gather | solution.py:69
  804.7 28.3 %all-gather.17.cloned.1.call-done = bf16[768,2048]{1,0:T(8,128)(2,1)} async-done(((bf16[192,2048]{1,0:T(8,128)(2,1)}), bf16[768,2048]{1,0:T(8,128)(2,1)}) %all-gather.17.cloned.1.call-update) | async-done | bytes 3145744 | tf_op jit(solution)/shard_map/all_gather | solution.py:134
  833.0 10.2 %multiply_convert_fusion = bf16[768,2048]{1,0:T(8,128)(2,1)S(1)} fusion(bf16[768,2048]{1,0:T(8,128)(2,1)} %all-gather.17.cloned.1.call-done, bf16[2048,2048]{1,0:T(8,128)(2,1)} %all-gather.19.cloned.1.call-done), kind=kOutput, calls=%fused_computation.41 | convolution fusion | flops 6447169536 | bytes 14680064 | tf_op jit(solution)/shard_map/dot_general | solution.py:135
  843.2 8.1 convolution_convert_fusion
  851.3 38.0 %reduce-scatter.5.cloned.1.call-done = bf16[192,2048]{1,0:T(8,128)(2,1)} async-done(((bf16[768,2048]{1,0:T(8,128)(2,1)}), bf16[192,2048]{1,0:T(8,128)(2,1)}) %reduce-scatter.5.cloned.1.call-update) | async-done | bytes 786448 | tf_op jit(solution)/shard_map/reduce_scatter | solution.py:137
  (299 shorter events, 192.1 us)
Async XLA Ops:
  6.5 507.5 %copy-start = (bf16[2,2,128,2048]{3,2,1,0:T(8,128)(2,1)S(1)}, bf16[2,2,128,2048]{3,2,1,0:T(8,128)(2,1)}, u32[]{:S(2)}) copy-start(bf16[2,2,128,2048]{3,2,1,0:T(8,128)(2,1)} %param.23) | copy-start | bytes 6291460
  6.5 65.8 %all-gather.9.cloned.1.call-start = ((), (), s32[]{:S(2)}) async-start(), calls=%async_computation.2 | async-start | bytes 3538944 | tf_op jit(solution)/shard_map/all_gather | solution.py:90
  8.5 124.7 %all-gather.11.cloned.1.call-start = ((), (), s32[]{:S(2)}) async-start(), calls=%async_computation.3 | async-start | bytes 3538944 | tf_op jit(solution)/shard_map/all_gather | solution.py:92
  10.4 183.7 %all-gather.15.cloned.1.call-start = ((), (), s32[]{:S(2)}) async-start(), calls=%async_computation.5 | async-start | bytes 3538944 | tf_op jit(solution)/shard_map/all_gather | solution.py:93
  11.3 282.2 %all-gather.13.cloned.1.call-start = ((), (), s32[]{:S(2)}) async-start(), calls=%async_computation.4 | async-start | bytes 7077888 | tf_op jit(solution)/shard_map/all_gather | solution.py:91
  12.4 541.0 %reduce-scatter.3.cloned.1.call-start = ((), (), s32[]{:S(2)}) async-start(), calls=%async_computation.6 | async-start | bytes 3932160 | tf_op jit(solution)/shard_map/reduce_scatter | solution.py:125
  332.5 8.6 slice-start
  332.5 8.6 slice-start.1
  359.5 8.6 slice-start
  359.5 8.6 slice-start.1
  386.5 8.6 slice-start
  386.5 8.6 slice-start.1
  413.5 8.6 slice-start
  413.5 8.6 slice-start.1
  440.6 8.6 slice-start
  467.6 8.6 slice-start
  494.6 8.6 slice-start
  494.6 8.6 slice-start.1
  517.2 36.2 %copy-start.6 = (bf16[192,2048]{1,0:T(8,128)(2,1)S(1)}, bf16[192,2048]{1,0:T(8,128)(2,1)}, u32[]{:S(2)}) copy-start(bf16[192,2048]{1,0:T(8,128)(2,1)} %param.24) | copy-start | bytes 2359300
  517.2 162.7 %all-gather.21.cloned.1.call-start = ((), (), s32[]{:S(2)}) async-start(), calls=%async_computation.10 | async-start | bytes 9437184 | tf_op jit(solution)/shard_map/all_gather | solution.py:12
  517.8 286.9 %all-gather.19.cloned.1.call-start = ((), (), s32[]{:S(2)}) async-start(), calls=%async_computation.8 | async-start | bytes 9437184 | tf_op jit(solution)/shard_map/all_gather | solution.py:69
  518.6 314.4 %all-gather.17.cloned.1.call-start = ((), (), s32[]{:S(2)}) async-start(), calls=%async_computation.7 | async-start | bytes 3932160 | tf_op jit(solution)/shard_map/all_gather | solution.py:134
  556.6 332.7 %reduce-scatter.5.cloned.1.call-start = ((), (), s32[]{:S(2)}) async-start(), calls=%async_computation.9 | async-start | bytes 3932160 | tf_op jit(solution)/shard_map/reduce_scatter | solution.py:137
  833.0 10.2 %copy-start.8 = (bf16[2048,8,256]{0,2,1:T(8,128)(2,1)S(1)}, bf16[2048,8,256]{0,2,1:T(8,128)(2,1)}, u32[]{:S(2)}) copy-start(bf16[2048,8,256]{0,2,1:T(8,128)(2,1)} %copy.55) | copy-start | bytes 25165828
  (48 other events, 180.8 us)
Sparse Core Ops, SparseCore 0:
  9.5 62.7 all-gather.8
  74.5 58.6 all-gather.10
  135.4 58.6 all-gather.14
  196.2 97.3 all-gather.12
  517.3 36.0 reduce-scatter.2
  555.4 124.4 all-gather.20
  682.0 122.6 all-gather.18
  806.3 26.6 all-gather.16
  851.4 37.8 reduce-scatter.4
